TPU v7x, 256 devices: a whole 4x4x8 slice. The times are simulated.
256 devices in a mesh: sp: 32 (over z, y), tp: 8 (over x, core).
Axes of the slice: x: 4, y: 4, z: 8, core: 2. Of those that a mesh axis runs over, the one named last changes fastest.
Arguments:
- query_a: bfloat16 [6144, 2048], P('sp', 'tp'), may hold values from -7.5 to 7.5
- key_a: bfloat16 [6144, 1024], P('sp', 'tp'), may hold values from -7.5 to 7.5
- value_a: bfloat16 [6144, 1024], P('sp', 'tp'), may hold values from -6 to 6
- query_b: bfloat16 [6144, 2048], P('sp', 'tp'), may hold values from -7.5 to 7.5
- key_b: bfloat16 [6144, 512], P('sp', 'tp'), may hold values from -7.5 to 7.5
- value_b: bfloat16 [6144, 512], P('sp', 'tp'), may hold values from -6 to 6
- gain_a: float32 [2, 128], replicated, may hold values from 1 to 6.5
- gain_b: float32 [2, 64], replicated, may hold values from 1 to 8.5
- out_a: bfloat16 [2048, 4096], P('tp'), may hold values from -0.5 to 0.5
- out_b: bfloat16 [2048, 4096], P('tp'), may hold values from -0.5 to 0.5
- residual: bfloat16 [6144, 4096], P('sp'), may hold values from -6 to 6
- norm_gain: float32 [4096], replicated, may hold values from 0.1 to 1.9
- gate_weight: bfloat16 [4096, 6144], P('sp', 'tp'), may hold values from -0.09375 to 0.09375
- up_weight: bfloat16 [4096, 6144], P('sp', 'tp'), may hold values from -0.09375 to 0.09375
- down_weight: bfloat16 [6144, 4096], P('tp', 'sp'), may hold values from -0.3125 to 0.3125
Outputs:
- output: bfloat16 [6144, 4096], P(('sp', 'tp'))
All inputs are finite; a program needn't handle non-finite values.
Results may differ from a plain program's by a relative error of at most 0.017.
The roundings to bfloat16 on the way count: a program that leaves them out, or rounds other values in their place, can miss the bound.
Values may be sent and summed in bfloat16 or wider, within the bound.
No kernel may reach another device: no remote copies, remote signals or barrier semaphores. Data moves between devices by JAX's collectives and lax.ppermute only.
A program may use at most 128 MiB of HBM per device.

v0:
```python
import jax
import jax.numpy as jnp
from jax import lax
from jax.sharding import PartitionSpec as P

HEAD_A = 128
HEAD_B = 64
GRID_W = 64
epsilon = 1e-06
theta_base = 10000.0


def rows_first(arrays, axis, dims):
    turned = [jnp.moveaxis(a, dim, 0) for a, dim in zip(arrays, dims)]
    both = jnp.concatenate([t.reshape(len(t), -1) for t in turned], axis=1)
    filled, at, outs = (lax.all_gather(both, axis, axis=0, tiled=True), 0, [])
    for t, dim in zip(turned, dims):
        share = filled[:, at : at + t[0].size].reshape(-1, *t.shape[1:])
        outs.append(jnp.moveaxis(share, 0, dim))
        at += t[0].size
    return tuple(outs)


def side_by_side(arrays, axis, dim, along):
    widths = [a.shape[along] for a in arrays]
    both = jnp.concatenate(arrays, axis=along)
    filled = lax.all_gather(both, axis, axis=dim, tiled=True)
    return tuple(jnp.split(filled, [sum(widths[:k]) for k in range(1, len(widths))], axis=along))


def cut_along(value, dim, devices):
    dims = value.shape
    parts = value.reshape(*dims[:dim], devices, dims[dim] // devices, *dims[dim + 1 :])
    return jnp.moveaxis(parts, dim, 0)


def sum_at_owner(value, axis, dim):
    parts = cut_along(value, dim, lax.axis_size(axis))
    arrived = lax.all_to_all(parts, axis, split_axis=0, concat_axis=0, tiled=True)
    return arrived.astype(jnp.float32).sum(axis=0)


def copy_for_each(value, axis):
    devices = lax.axis_size(axis)
    return lax.all_to_all(
        jnp.broadcast_to(value[None], (devices, *value.shape)), axis, 0, 0, tiled=True
    )


def laid_out(parts, dim):
    dims = list(parts.shape[1:])
    dims[dim] *= parts.shape[0]
    return jnp.moveaxis(parts, 0, dim).reshape(dims)


def gathered_copies(value, axis, dim):
    parts = copy_for_each(value, axis)
    return laid_out(parts, dim)


def rotate(inputs, num_heads, head_size, first_pos, gain):
    tok_rows = inputs.shape[0]
    vectors = inputs.astype(jnp.float32).reshape(tok_rows, num_heads, head_size)
    vectors = (
        vectors * lax.rsqrt(jnp.mean(vectors * vectors, axis=-1, keepdims=True) + epsilon) * gain
    )
    position = first_pos + jnp.arange(tok_rows, dtype=jnp.int32)
    grid_row = (position // GRID_W).astype(jnp.float32)
    grid_col = (position % GRID_W).astype(jnp.float32)
    quarter = head_size // 4
    inv_freq = theta_base ** (-4.0 * jnp.arange(quarter, dtype=jnp.float32) / head_size)
    angle_row = grid_row[:, None] * inv_freq[None, :]
    angle_col = grid_col[:, None] * inv_freq[None, :]
    angles = jnp.concatenate([angle_row, angle_row, angle_col, angle_col], axis=-1)
    quarters = vectors.reshape(tok_rows, num_heads, 4, quarter)
    rotated = jnp.stack(
        [-quarters[:, :, 1], quarters[:, :, 0], -quarters[:, :, 3], quarters[:, :, 2]], axis=2
    )
    rotated = rotated.reshape(tok_rows, num_heads, head_size)
    result = vectors * jnp.cos(angles)[:, None, :] + rotated * jnp.sin(angles)[:, None, :]
    return result.reshape(tok_rows, num_heads * head_size).astype(jnp.bfloat16)


def start_state(kv_heads, groups, tok_rows, head_size):
    return (
        jnp.full((kv_heads, groups, tok_rows), -1e30, jnp.float32),
        jnp.zeros((kv_heads, groups, tok_rows), jnp.float32),
        jnp.zeros((kv_heads, groups, tok_rows, head_size), jnp.float32),
    )


def attend(state, queries, key_rows, values, head_size):
    run_max, run_sum, run_acc = state
    kv_heads = key_rows.shape[1] // head_size
    groups = run_max.shape[1]
    q_heads = queries.reshape(queries.shape[0], kv_heads, groups, head_size)
    k_heads = key_rows.reshape(key_rows.shape[0], kv_heads, head_size)
    v_heads = values.reshape(values.shape[0], kv_heads, head_size)
    scores = jnp.einsum(
        "tkgd,pkd->kgtp", q_heads, k_heads, preferred_element_type=jnp.float32
    ) * head_size ** (-0.5)
    new_max = jnp.maximum(run_max, jnp.max(scores, axis=-1))
    exp_scores = jnp.exp(scores - new_max[..., None])
    new_sum = jnp.sum(exp_scores, axis=-1)
    new_acc = jnp.einsum(
        "kgtp,pkd->kgtd",
        exp_scores.astype(jnp.bfloat16),
        v_heads,
        preferred_element_type=jnp.float32,
    )
    return (new_max, new_sum, new_acc)


def finish(state, num_cols):
    blended = state[2] / state[1][..., None]
    return blended.transpose(2, 0, 1, 3).reshape(blended.shape[2], num_cols).astype(jnp.bfloat16)


def normalize(mixed_rows, gain):
    scale = lax.rsqrt(jnp.mean(mixed_rows * mixed_rows, axis=-1, keepdims=True) + epsilon)
    return (mixed_rows * scale * gain).astype(jnp.bfloat16)


def on_device(
    query_a,
    key_a,
    value_a,
    query_b,
    key_b,
    value_b,
    gain_a,
    gain_b,
    out_a,
    out_b,
    residual,
    norm_gain,
    gate_weight,
    up_weight,
    down_weight,
):
    tok_rows = query_a.shape[0]
    first_pos = lax.axis_index("sp") * tok_rows
    heads_a = query_a.shape[1] // HEAD_A
    heads_b = query_b.shape[1] // HEAD_B
    kv_heads_a = key_a.shape[1] // HEAD_A
    kv_heads_b = key_b.shape[1] // HEAD_B
    kv_width_b = kv_heads_b * HEAD_B
    turned_qa = rotate(query_a, heads_a, HEAD_A, first_pos, gain_a[0])
    turned_ka = rotate(key_a, kv_heads_a, HEAD_A, first_pos, gain_a[1])
    turned_qb = rotate(query_b, heads_b, HEAD_B, first_pos, gain_b[0])
    turned_kb = rotate(key_b, kv_heads_b, HEAD_B, first_pos, gain_b[1])
    pair_b = jnp.concatenate([turned_kb, value_b], axis=1)
    gate_full, up_full, down_full = rows_first(
        (gate_weight, up_weight, down_weight), "sp", (0, 0, 1)
    )
    initial = (
        start_state(kv_heads_a, heads_a // kv_heads_a, tok_rows, HEAD_A),
        start_state(kv_heads_b, heads_b // kv_heads_b, tok_rows, HEAD_B),
    )
    pieces = side_by_side((turned_ka, value_a, pair_b), "sp", 0, 1)
    state_a = attend(initial[0], turned_qa, pieces[0], pieces[1], HEAD_A)
    state_b = attend(
        initial[1], turned_qb, pieces[2][:, :kv_width_b], pieces[2][:, kv_width_b:], HEAD_B
    )
    attn_a = finish(state_a, query_a.shape[1])
    attn_b = finish(state_b, query_b.shape[1])
    own_rows = tok_rows // lax.axis_size("tp")
    own_start = lax.axis_index("tp") * own_rows
    head_sum = sum_at_owner(
        (
            jnp.dot(attn_a, out_a, preferred_element_type=jnp.float32)
            + jnp.dot(attn_b, out_b, preferred_element_type=jnp.float32)
        ).astype(jnp.bfloat16),
        "tp",
        0,
    )
    own_resid = lax.dynamic_slice_in_dim(residual, own_start, own_rows, 0)
    mixed_rows = own_resid.astype(jnp.float32) + head_sum
    normed = gathered_copies(normalize(mixed_rows, norm_gain), "tp", 0)
    gate_act = jnp.dot(normed, gate_full, preferred_element_type=jnp.float32)
    up_act = jnp.dot(normed, up_full, preferred_element_type=jnp.float32)
    hidden = (jax.nn.silu(gate_act) * up_act).astype(jnp.bfloat16)
    branch_sum = sum_at_owner(
        jnp.dot(hidden, down_full, preferred_element_type=jnp.float32).astype(jnp.bfloat16), "tp", 0
    )
    return (mixed_rows + 0.5 * branch_sum).astype(jnp.bfloat16)


def solution(mesh):
    return jax.shard_map(
        on_device,
        mesh=mesh,
        in_specs=(
            P("sp", "tp"),
            P("sp", "tp"),
            P("sp", "tp"),
            P("sp", "tp"),
            P("sp", "tp"),
            P("sp", "tp"),
            P(),
            P(),
            P("tp", None),
            P("tp", None),
            P("sp", None),
            P(),
            P("sp", "tp"),
            P("sp", "tp"),
            P("tp", "sp"),
        ),
        out_specs=P(("sp", "tp"), None),
        check_vma=False,
    )
```

profile of v0, /device:TPU:1, one launch (start us, length us, event | category | flops | bytes accessed | tf_op | source)
XLA Modules:
  0.0 315.2 jit_solution(1627057619854827771)
XLA Ops:
  14.1 1.3 add_convert_fusion.1
  15.3 1.6 pad_maximum_fusion.3
  17.0 1.1 copy.54
  18.0 1.1 copy.55
  19.1 1.8 pad_maximum_fusion
  22.3 77.9 %all-gather.3.cloned.1.call-done = bf16[6144,384]{1,0:T(8,128)(2,1)} async-done(((bf16[192,384]{1,0:T(8,128)(2,1)}), bf16[6144,384]{1,0:T(8,128)(2,1)}) %all-gather.3.cloned.1.call-update) | async-done | bytes 4718608 | tf_op jit(solution)/shard_map/all_gather | solution.py:27
  100.2 2.9 bitcast_reduce_fusion.1
  103.1 1.4 fusion.7
  105.5 1.4 fusion.38
  107.0 8.0 %bitcast_reduce_fusion = (f32[4,192]{1,0:T(4,128)S(1)}, f32[6144,192,4]{0,1,2:T(8,128)}) fusion(bf16[192,4,64]{0,2,1:T(8,128)(2,1)S(1)} %bitcast.178, bf16[6144,384]{1,0:T(8,128)(2,1)S(1)} %copy-done.3), kind=kOutput, calls=%fused_computation.1 | convolution fusion | flops 613416192 | bytes 20581376 | tf_op jit(solution)/shard_map/tkgd,pkd->kgtp/dot_general | solution.py:99
  115.1 2.2 fusion.61
  117.3 9.7 %fusion.1 = f32[4,192]{1,0:T(4,128)S(1)} fusion(f32[6144,192,4]{0,1,2:T(8,128)} %get-tuple-element.40, f32[4,192]{1,0:T(4,128)S(1)} %broadcast_maximum_fusion), kind=kLoop, calls=%fused_computation.3 | loop fusion | flops 14155008 | bytes 18880512 | tf_op jit(solution)/shard_map/reduce_sum | solution.py:104
  127.0 10.7 %fusion.44 = bf16[4,192,64]{1,2,0:T(8,128)(2,1)S(1)} fusion(bf16[6144,384]{1,0:T(8,128)(2,1)} %all-gather.3.cloned.1.call-done, f32[6144,192,4]{0,1,2:T(8,128)} %get-tuple-element.40, f32[4,192]{1,0:T(4,128)S(1)} %broadcast_maximum_fusion, f32[4,192]{1,0:T(4,128)S(1)} %fusion.1), kind=kOutput, calls=%fused_computation.38 | convolution fusion | flops 618233856 | bytes 20551680 | tf_op jit(solution)/shard_map/kgtp,pkd->kgtd/dot_general | solution.py:105
  137.7 1.8 fusion.15
  139.5 9.0 %all-to-all-start = ((bf16[8,24,4096]{2,1,0:T(8,128)(2,1)}), bf16[8,24,4096]{2,1,0:T(8,128)(2,1)S(1)}, u32[]{:S(2)}, u32[]{:S(2)}) async-start(bf16[8,24,4096]{2,1,0:T(8,128)(2,1)} %bitcast.171), calls=%async_computation | async-start | bytes 3145728 | tf_op jit(solution)/shard_map/all_to_all | solution.py:39
  148.5 20.6 %all-to-all-done = bf16[8,24,4096]{2,1,0:T(8,128)(2,1)S(1)} async-done(((bf16[8,24,4096]{2,1,0:T(8,128)(2,1)}), bf16[8,24,4096]{2,1,0:T(8,128)(2,1)S(1)}, u32[]{:S(2)}, u32[]{:S(2)}) %all-to-all-start) | async-done | bytes 1572896 | tf_op jit(solution)/shard_map/all_to_all | solution.py:39
  169.3 1.1 multiply_reduce_fusion
  170.4 1.1 multiply_convert_fusion
  171.7 24.7 %all_to_all.15 = bf16[8,24,4096]{2,1,0:T(8,128)(2,1)} all-to-all(bf16[8,24,4096]{2,1,0:T(8,128)(2,1)S(1)} %broadcast_in_dim.8), channel_id=1, replica_groups=mesh['sp'=32,'tp'=8] {'tp'}, dimensions={0} | all-to-all | bytes 3145728 | tf_op jit(solution)/shard_map/all_to_all | solution.py:45
  196.3 65.0 %all-gather.5.cloned.1.call-done = bf16[4096,2304]{0,1:T(8,128)(2,1)} async-done(((bf16[128,2304]{0,1:T(8,128)(2,1)}), bf16[4096,2304]{0,1:T(8,128)(2,1)}) %all-gather.5.cloned.1.call-update) | async-done | bytes 18874384 | tf_op jit(solution)/shard_map/all_gather | solution.py:16
  261.3 5.5 %fusion.13 = f32[192,768]{1,0:T(8,128)S(1)} fusion(bf16[192,4096]{1,0:T(8,128)(2,1)} %bitcast.174, bf16[4096,2304]{0,1:T(8,128)(2,1)} %all-gather.5.cloned.1.call-done), kind=kOutput, calls=%fused_computation.17 | convolution fusion | flops 1207959552 | bytes 8454144 | tf_op jit(solution)/shard_map/dot_general | solution.py:180
  266.8 10.9 %fusion.16 = bf16[192,4096]{1,0:T(8,128)(2,1)} fusion(bf16[4096,2304]{0,1:T(8,128)(2,1)} %all-gather.5.cloned.1.call-done, bf16[192,4096]{1,0:T(8,128)(2,1)} %bitcast.175, f32[192,768]{1,0:T(8,128)S(1)} %fusion.13), kind=kOutput, calls=%fused_computation.21 | convolution fusion | flops 2417590272 | bytes 16318464 | tf_op jit(solution)/shard_map/dot_general | solution.py:184
  277.7 28.8 %all_to_all.16 = bf16[8,24,4096]{2,1,0:T(8,128)(2,1)S(1)} all-to-all(bf16[8,24,4096]{2,1,0:T(8,128)(2,1)} %bitcast.176), channel_id=1, replica_groups=mesh['sp'=32,'tp'=8] {'tp'}, dimensions={0} | all-to-all | bytes 3145728 | tf_op jit(solution)/shard_map/all_to_all | solution.py:39
  306.7 1.7 add_convert_fusion
  (70 shorter events, 10.4 us)
Async XLA Ops:
  6.5 108.5 %copy-start = (bf16[256,4096]{1,0:T(8,128)(2,1)S(1)}, bf16[256,4096]{1,0:T(8,128)(2,1)}, u32[]{:S(2)}) copy-start(bf16[256,4096]{1,0:T(8,128)(2,1)} %param.23) | copy-start | bytes 6291460
  6.5 14.4 %copy-start.5 = (bf16[192,256]{1,0:T(8,128)(2,1)S(1)}, bf16[192,256]{1,0:T(8,128)(2,1)}, u32[]{:S(2)}) copy-start(bf16[192,256]{1,0:T(8,128)(2,1)} %param.18) | copy-start | bytes 294916
  6.5 14.9 %copy-start.6 = (bf16[192,256]{1,0:T(8,128)(2,1)S(1)}, bf16[192,256]{1,0:T(8,128)(2,1)}, u32[]{:S(2)}) copy-start(bf16[192,256]{1,0:T(8,128)(2,1)} %param.15) | copy-start | bytes 294916
  6.5 93.6 %all-gather.3.cloned.1.call-start = ((), (), s32[]{:S(2)}) async-start(), calls=%async_computation.3 | async-start | bytes 4866048 | tf_op jit(solution)/shard_map/all_gather | solution.py:27
  16.9 244.4 %all-gather.5.cloned.1.call-start = ((), (), s32[]{:S(2)}) async-start(), calls=%async_computation.4 | async-start | bytes 19464192 | tf_op jit(solution)/shard_map/all_gather | solution.py:16
  103.1 2.3 copy-start.3
  127.0 10.7 %copy-start.2 = (f32[192,4096]{1,0:T(8,128)S(1)}, f32[192,4096]{1,0:T(8,128)}, u32[]{:S(2)}) copy-start(f32[192,4096]{1,0:T(8,128)} %fusion.61) | copy-start | bytes 9437188
  127.0 10.7 %copy-start.4 = (bf16[256,4096]{1,0:T(8,128)(2,1)S(1)}, bf16[256,4096]{1,0:T(8,128)(2,1)}, u32[]{:S(2)}) copy-start(bf16[256,4096]{1,0:T(8,128)(2,1)} %param.24) | copy-start | bytes 6291460
  137.7 32.7 %copy-start.7 = (f32[4096]{0:T(1024)S(1)}, f32[4096]{0:T(1024)}, u32[]{:S(2)}) copy-start(f32[4096]{0:T(1024)} %param.26) | copy-start | bytes 49156
  139.5 29.6 %all-to-all-start = ((bf16[8,24,4096]{2,1,0:T(8,128)(2,1)}), bf16[8,24,4096]{2,1,0:T(8,128)(2,1)S(1)}, u32[]{:S(2)}, u32[]{:S(2)}) async-start(bf16[8,24,4096]{2,1,0:T(8,128)(2,1)} %bitcast.171), calls=%async_computation | async-start | bytes 3145728 | tf_op jit(solution)/shard_map/all_to_all | solution.py:39
  266.8 41.6 %copy-start.1 = (bf16[256,4096]{1,0:T(8,128)(2,1)S(1)}, bf16[256,4096]{1,0:T(8,128)(2,1)}, u32[]{:S(2)}) copy-start(bf16[256,4096]{1,0:T(8,128)(2,1)} %param.23) | copy-start | bytes 6291460
Sparse Core Ops, SparseCore 0:
  17.0 83.1 all-gather.2
  102.6 158.6 all-gather.4
where the time goes:
time: 316 us; the launch traced here: 315 us
  waiting for transfers between devices  163 us (52%)
  blocking collectives  53.4 us (17%)
  matrix products  43.4 us (14%)
  other arithmetic  25.2 us (8%)
  between operations  13.8 us (4%)
  starting transfers between devices  9.09 us (3%)
  local copies, waits for them, and re-layouts  6.82 us (2%)
    all_gather x1, waiting for transfers between devices, side_by_side(): filled = lax.all_gather(both, axis, axis=dim, tiled=True)  77.9 us
    all_gather x1, waiting for transfers between devices, rows_first(): filled, at, outs = (lax.all_gather(both, axis, axis=0, tiled=True), 0, [])  65 us
    all_to_all x1, blocking collectives, sum_at_owner(): lax.all_to_all(parts, axis, split_axis=0, concat_axis=0, tiled=True)  28.8 us
    all_to_all x1, blocking collectives, copy_for_each(): lax.all_to_all(jnp.broadcast_to(value[None], (devices, *value.shape)), ax...  24.7 us
    all_to_all x1, waiting for transfers between devices, sum_at_owner(): lax.all_to_all(parts, axis, split_axis=0, concat_axis=0, tiled=True)  20.6 us
    dot_general x2, matrix products, attend(): jnp.einsum('kgtp,pkd->kgtd', exp_scores.astype(jnp.bfloat16), v_heads, pr...  12.1 us
    reduce_sum x2, other arithmetic, attend(): new_sum = jnp.sum(exp_scores, axis=-1)  11.1 us
    dot_general x2, matrix products, attend(): jnp.einsum('tkgd,pkd->kgtp', q_heads, k_heads, preferred_element_type=jnp...  11 us
  transfers between devices with their start and end apart: 3, of which 3 were waited for; matrix products, arithmetic and copies ran while one was open for 15% of the time, Pallas kernels for 0%

commit v1 on v0

--- a/solution.py
+++ b/solution.py
@@ -10,10 +10,17 @@
 theta_base = 10000.0
 
 
+def gather_over(value, name, dim):
+    size = lax.axis_size(name)
+    shards = jnp.stack([value for _ in range(size)])
+    shards = lax.all_to_all(shards, name, split_axis=0, concat_axis=0)
+    return jnp.concatenate(shards, axis=dim)
+
+
 def rows_first(arrays, axis, dims):
     turned = [jnp.moveaxis(a, dim, 0) for a, dim in zip(arrays, dims)]
     both = jnp.concatenate([t.reshape(len(t), -1) for t in turned], axis=1)
-    filled, at, outs = (lax.all_gather(both, axis, axis=0, tiled=True), 0, [])
+    filled, at, outs = (gather_over(both, axis, 0), 0, [])
     for t, dim in zip(turned, dims):
         share = filled[:, at : at + t[0].size].reshape(-1, *t.shape[1:])
         outs.append(jnp.moveaxis(share, 0, dim))

time: 316 us -> 667 us (2.11)
  blocking collectives: 53.4 us -> 440 us
  waiting for transfers between devices: 163 us -> 121 us
  local copies, waits for them, and re-layouts: 6.82 us -> 15.9 us
    all_to_all x1, blocking collectives: 24.7 us -> 413 us  [gather_over(): shards = lax.all_to_all(shards, name, split_axis=0, concat_axis=0)]
    all_gather x1 -> x0, waiting for transfers between devices: 65 us -> none  [rows_first(): filled, at, outs = (lax.all_gather(both, axis, axis=0, tiled=True), 0, [])]
    all_to_all x0 -> x1, waiting for transfers between devices: none -> 20.1 us  [copy_for_each(): lax.all_to_all(jnp.broadcast_to(value[None], (devices, *value.shape)), ax...]
  transfers between devices with their start and end apart: 3 -> 3, of which waited for: 3 -> 3; matrix products, arithmetic and copies ran while one was open for 15% -> 1% of each run, Pallas kernels for 0% -> 0%
where the time goes in v1:
time: 667 us; the launch traced here: 666 us
  blocking collectives  440 us (66%)
  waiting for transfers between devices  121 us (18%)
  matrix products  38.6 us (6%)
  other arithmetic  23.3 us (3%)
  local copies, waits for them, and re-layouts  15.9 us (2%)
  starting transfers between devices  13.8 us (2%)
  between operations  13.7 us (2%)
    all_to_all x1, blocking collectives, gather_over(): shards = lax.all_to_all(shards, name, split_axis=0, concat_axis=0)  413 us
    all_gather x1, waiting for transfers between devices, side_by_side(): filled = lax.all_gather(both, axis, axis=dim, tiled=True)  80.1 us
    all_to_all x1, blocking collectives, sum_at_owner(): lax.all_to_all(parts, axis, split_axis=0, concat_axis=0, tiled=True)  27 us
    all_to_all x1, waiting for transfers between devices, sum_at_owner(): lax.all_to_all(parts, axis, split_axis=0, concat_axis=0, tiled=True)  20.6 us
    all_to_all x1, waiting for transfers between devices, copy_for_each(): lax.all_to_all(jnp.broadcast_to(value[None], (devices, *value.shape)), ax...  20.1 us
  transfers between devices with their start and end apart: 3, of which 3 were waited for; matrix products, arithmetic and copies ran while one was open for 1% of the time, Pallas kernels for 0%

profile of v1, /device:TPU:1, one launch (start us, length us, event | category | flops | bytes accessed | tf_op | source)
XLA Modules:
  0.0 666.4 jit_solution(18058287617744468619)
XLA Ops:
  14.0 1.3 add_convert_fusion.1
  15.3 1.6 pad_maximum_fusion.3
  20.0 80.1 %all-gather.2.cloned.1.call-done = bf16[6144,384]{1,0:T(8,128)(2,1)} async-done(((bf16[192,384]{1,0:T(8,128)(2,1)}), bf16[6144,384]{1,0:T(8,128)(2,1)}) %all-gather.2.cloned.1.call-update) | async-done | bytes 4718608 | tf_op jit(solution)/shard_map/all_gather | solution.py:34
  100.2 9.5 %bitcast_reduce_fusion = (f32[4,192]{1,0:T(4,128)S(1)}, f32[6144,192,4]{0,1,2:T(8,128)}) fusion(bf16[192,4,64]{0,2,1:T(8,128)(2,1)S(1)} %bitcast.179, bf16[6144,384]{1,0:T(8,128)(2,1)} %all-gather.2.cloned.1.call-done), kind=kOutput, calls=%fused_computation.1 | convolution fusion | flops 613416192 | bytes 20548608 | tf_op jit(solution)/shard_map/tkgd,pkd->kgtp/dot_general | solution.py:106
  109.6 1.5 bitcast_reduce_fusion.1
  111.2 1.4 fusion.7
  112.6 1.4 fusion.38
  114.2 9.5 %fusion.1 = f32[4,192]{1,0:T(4,128)S(1)} fusion(f32[6144,192,4]{0,1,2:T(8,128)} %get-tuple-element.40, f32[4,192]{1,0:T(4,128)S(1)} %broadcast_maximum_fusion), kind=kLoop, calls=%fused_computation.3 | loop fusion | flops 14155008 | bytes 18880512 | tf_op jit(solution)/shard_map/reduce_sum | solution.py:111
  124.3 10.5 %fusion.44 = bf16[4,192,64]{1,2,0:T(8,128)(2,1)S(1)} fusion(bf16[6144,384]{1,0:T(8,128)(2,1)} %all-gather.2.cloned.1.call-done, f32[6144,192,4]{0,1,2:T(8,128)} %get-tuple-element.40, f32[4,192]{1,0:T(4,128)S(1)} %broadcast_maximum_fusion, f32[4,192]{1,0:T(4,128)S(1)} %fusion.1), kind=kOutput, calls=%fused_computation.38 | convolution fusion | flops 618233856 | bytes 20551680 | tf_op jit(solution)/shard_map/kgtp,pkd->kgtd/dot_general | solution.py:112
  134.8 2.0 fusion.15
  136.9 8.6 %all-to-all-start = ((bf16[8,24,4096]{2,1,0:T(8,128)(2,1)}), bf16[8,24,4096]{2,1,0:T(8,128)(2,1)S(1)}, u32[]{:S(2)}, u32[]{:S(2)}) async-start(bf16[8,24,4096]{2,1,0:T(8,128)(2,1)} %bitcast.174), calls=%async_computation | async-start | bytes 3145728 | tf_op jit(solution)/shard_map/all_to_all | solution.py:46
  145.5 20.6 %all-to-all-done = bf16[8,24,4096]{2,1,0:T(8,128)(2,1)S(1)} async-done(((bf16[8,24,4096]{2,1,0:T(8,128)(2,1)}), bf16[8,24,4096]{2,1,0:T(8,128)(2,1)S(1)}, u32[]{:S(2)}, u32[]{:S(2)}) %all-to-all-start) | async-done | bytes 1572896 | tf_op jit(solution)/shard_map/all_to_all | solution.py:46
  166.3 1.1 multiply_reduce_fusion
  167.4 1.0 multiply_convert_fusion
  168.4 1.3 broadcast_in_dim.8
  169.8 5.1 all-to-all-start.1
  175.6 20.1 %all-to-all-done.1 = bf16[8,24,4096]{2,1,0:T(8,128)(2,1)} async-done(((bf16[8,24,4096]{2,1,0:T(8,128)(2,1)}), bf16[8,24,4096]{2,1,0:T(8,128)(2,1)}, u32[]{:S(2)}, u32[]{:S(2)}) %all-to-all-start.1) | async-done | bytes 1572896 | tf_op jit(solution)/shard_map/all_to_all | solution.py:52
  195.6 2.2 stack.14
  197.8 413.3 %all_to_all.20 = bf16[32,128,2304]{2,1,0:T(8,128)(2,1)S(1)} all-to-all(bf16[32,128,2304]{2,1,0:T(8,128)(2,1)S(1)} %stack.14), channel_id=1, replica_groups=mesh['sp'=32,'tp'=8] {'sp'}, dimensions={0} | all-to-all | bytes 37748736 | tf_op jit(solution)/shard_map/all_to_all | solution.py:16
  611.1 6.5 copy-done.2
  617.5 2.8 fusion.13
  620.4 10.2 %fusion.16 = bf16[192,4096]{1,0:T(8,128)(2,1)} fusion(bf16[4096,2304]{1,0:T(8,128)(2,1)} %bitcast.173, bf16[192,4096]{1,0:T(8,128)(2,1)} %bitcast.41, f32[192,768]{1,0:T(8,128)S(1)} %fusion.13), kind=kOutput, calls=%fused_computation.21 | convolution fusion | flops 2417590272 | bytes 16318464 | tf_op jit(solution)/shard_map/dot_general | solution.py:191
  630.6 27.0 %all_to_all.21 = bf16[8,24,4096]{2,1,0:T(8,128)(2,1)S(1)} all-to-all(bf16[8,24,4096]{2,1,0:T(8,128)(2,1)} %bitcast.177), channel_id=1, replica_groups=mesh['sp'=32,'tp'=8] {'tp'}, dimensions={0} | all-to-all | bytes 3145728 | tf_op jit(solution)/shard_map/all_to_all | solution.py:46
  657.8 1.7 add_convert_fusion
  (73 shorter events, 12.2 us)
Async XLA Ops:
  6.5 117.2 %copy-start = (bf16[256,4096]{1,0:T(8,128)(2,1)S(1)}, bf16[256,4096]{1,0:T(8,128)(2,1)}, u32[]{:S(2)}) copy-start(bf16[256,4096]{1,0:T(8,128)(2,1)} %param.23) | copy-start | bytes 6291460
  6.5 93.6 %all-gather.2.cloned.1.call-start = ((), (), s32[]{:S(2)}) async-start(), calls=%async_computation.4 | async-start | bytes 4866048 | tf_op jit(solution)/shard_map/all_gather | solution.py:34
  100.2 9.5 %copy-start.3 = (bf16[6144,384]{1,0:T(8,128)(2,1)S(1)}, bf16[6144,384]{1,0:T(8,128)(2,1)}, u32[]{:S(2)}) copy-start(bf16[6144,384]{1,0:T(8,128)(2,1)} %all-gather.2.cloned.1.call-done) | copy-start | bytes 14155780
  124.3 10.5 %copy-start.4 = (bf16[256,4096]{1,0:T(8,128)(2,1)S(1)}, bf16[256,4096]{1,0:T(8,128)(2,1)}, u32[]{:S(2)}) copy-start(bf16[256,4096]{1,0:T(8,128)(2,1)} %param.24) | copy-start | bytes 6291460
  134.8 32.6 %copy-start.8 = (f32[4096]{0:T(1024)S(1)}, f32[4096]{0:T(1024)}, u32[]{:S(2)}) copy-start(f32[4096]{0:T(1024)} %param.26) | copy-start | bytes 49156
  136.9 29.2 %all-to-all-start = ((bf16[8,24,4096]{2,1,0:T(8,128)(2,1)}), bf16[8,24,4096]{2,1,0:T(8,128)(2,1)S(1)}, u32[]{:S(2)}, u32[]{:S(2)}) async-start(bf16[8,24,4096]{2,1,0:T(8,128)(2,1)} %bitcast.174), calls=%async_computation | async-start | bytes 3145728 | tf_op jit(solution)/shard_map/all_to_all | solution.py:46
  145.5 29.4 %copy-start.6 = (bf16[128,768]{1,0:T(8,128)(2,1)S(1)}, bf16[128,768]{1,0:T(8,128)(2,1)}, u32[]{:S(2)}) copy-start(bf16[128,768]{1,0:T(8,128)(2,1)} %param.27) | copy-start | bytes 589828
  145.5 29.6 %copy-start.7 = (bf16[128,768]{1,0:T(8,128)(2,1)S(1)}, bf16[128,768]{1,0:T(8,128)(2,1)}, u32[]{:S(2)}) copy-start(bf16[128,768]{1,0:T(8,128)(2,1)} %param.28) | copy-start | bytes 589828
  145.5 29.8 %copy-start.5 = (bf16[768,128]{1,0:T(8,128)(2,1)S(1)}, bf16[768,128]{1,0:T(8,128)(2,1)}, u32[]{:S(2)}) copy-start(bf16[768,128]{1,0:T(8,128)(2,1)} %param.29) | copy-start | bytes 589828
  169.8 25.9 %all-to-all-start.1 = ((bf16[8,24,4096]{2,1,0:T(8,128)(2,1)}), bf16[8,24,4096]{2,1,0:T(8,128)(2,1)}, u32[]{:S(2)}, u32[]{:S(2)}) async-start(bf16[8,24,4096]{2,1,0:T(8,128)(2,1)} %broadcast_in_dim.8), calls=%async_computation.1 | async-start | bytes 3145728 | tf_op jit(solution)/shard_map/all_to_all | solution.py:52
  611.1 6.5 copy-start.2
  620.4 39.1 %copy-start.1 = (bf16[256,4096]{1,0:T(8,128)(2,1)S(1)}, bf16[256,4096]{1,0:T(8,128)(2,1)}, u32[]{:S(2)}) copy-start(bf16[256,4096]{1,0:T(8,128)(2,1)} %param.23) | copy-start | bytes 6291460
Sparse Core Ops, SparseCore 0:
  17.0 83.1 all-gather.1
